TPU v7x, 256 devices: a whole 4x4x8 slice. The times are simulated.
256 devices in a mesh: sp: 32 (over z, x), tp: 8 (over y, core).
Axes of the slice: x: 4, y: 4, z: 8, core: 2. Of those that a mesh axis runs over, the one named last changes fastest.
Arguments:
- features: bfloat16 [12288, 2048], P('sp', 'tp'), may hold values from -6 to 6
- norm_gain: float32 [2048], replicated, may hold values from 0.28 to 10
- w_query: bfloat16 [2048, 1024], P(None, 'tp'), may hold values from -0.125 to 0.125
- w_key: bfloat16 [2048, 512], P(None, 'tp'), may hold values from -0.125 to 0.125
- w_value: bfloat16 [2048, 512], P(None, 'tp'), may hold values from -0.125 to 0.125
- head_sinks: float32 [16], P('tp'), may hold values from 1 to 5
- w_query_latent: bfloat16 [2048, 512], replicated, may hold values from -0.125 to 0.125
- w_kv_latent: bfloat16 [2048, 512], replicated, may hold values from -0.125 to 0.125
- w_rope_key: bfloat16 [2048, 64], replicated, may hold values from -0.125 to 0.125
- query_latent_gain: float32 [512], replicated, may hold values from 0.28 to 10
- kv_latent_gain: float32 [512], replicated, may hold values from 0.28 to 10
- w_query_content: bfloat16 [512, 1024], P(None, 'tp'), may hold values from -0.25 to 0.25
- w_query_rotary: bfloat16 [512, 512], P(None, 'tp'), may hold values from -0.25 to 0.25
- w_key_up: bfloat16 [512, 1024], P(None, 'tp'), may hold values from -0.25 to 0.25
- w_value_up: bfloat16 [512, 1024], P(None, 'tp'), may hold values from -0.25 to 0.25
- w_branch_window: bfloat16 [1024, 2048], P('tp'), may hold values from -0.1875 to 0.1875
- w_branch_latent: bfloat16 [1024, 2048], P('tp'), may hold values from -0.1875 to 0.1875
- w_gate_window: bfloat16 [2048, 2048], P(None, 'tp'), may hold values from -0.125 to 0.125
- w_gate_latent: bfloat16 [2048, 2048], P(None, 'tp'), may hold values from -0.125 to 0.125
Outputs:
- mixed: bfloat16 [12288, 2048], P('sp', 'tp')
All inputs are finite; a program needn't handle non-finite values.
Results may differ from a plain program's by a relative error of at most 0.018.
The roundings to bfloat16 on the way count: a program that leaves them out, or rounds other values in their place, can miss the bound.
Values may be sent and summed in bfloat16 or wider, within the bound.
A program may use at most 128 MiB of HBM per device.

v0:
```python
import jax
import jax.numpy as jnp
from jax import lax
from jax.sharding import PartitionSpec as P

HEAD = 64
WINDOW = 128
NOPE = 128
ROPE = 64
VDIM = 128
EPS = 1e-06
THETA = 10000.0
NEGATIVE = -1e30


def copy_for_each(shard, axis):
    count = lax.axis_size(axis)
    return lax.all_to_all(
        jnp.broadcast_to(shard[None], (count, *shard.shape)), axis, 0, 0, tiled=True
    )


def in_order(parts, dim):
    shape = list(parts.shape[1:])
    shape[dim] *= parts.shape[0]
    return jnp.moveaxis(parts, 0, dim).reshape(shape)


def gathered_copies(shard, axis, dim):
    parts = copy_for_each(shard, axis)
    return in_order(parts, dim)


def from_behind(shard, axis, by):
    count = lax.axis_size(axis)
    pairs = [(i, i + by) for i in range(count) if 0 <= i + by < count]
    return lax.ppermute(shard, axis, pairs)


def in_one_piece(arrays, axis, dim, along):
    widths = [a.shape[along] for a in arrays]
    both = jnp.concatenate(arrays, axis=along)
    result = lax.all_gather(both, axis, axis=dim, tiled=True)
    return tuple(jnp.split(result, [sum(widths[:k]) for k in range(1, len(widths))], axis=along))


def rms_rows(float_rows, gain_vec):
    return (
        float_rows
        * lax.rsqrt(jnp.mean(float_rows * float_rows, axis=-1, keepdims=True) + EPS)
        * gain_vec
    )


def rotate(float_rows, positions):
    half_width = float_rows.shape[-1] // 2
    frequencies = THETA ** (-jnp.arange(half_width, dtype=jnp.float32) / half_width)
    angles = positions.astype(jnp.float32)[:, None] * frequencies
    target = (float_rows.shape[0],) + (1,) * (float_rows.ndim - 2) + (half_width,)
    cosine = jnp.cos(angles).reshape(target)
    sine_part = jnp.sin(angles).reshape(target)
    first_half = float_rows[..., :half_width]
    second_half = float_rows[..., half_width:]
    return jnp.concatenate(
        [
            first_half * cosine - second_half * sine_part,
            second_half * cosine + first_half * sine_part,
        ],
        axis=-1,
    )


def project(left, right):
    return jnp.dot(left, right, preferred_element_type=jnp.float32)


def window_attention(queries, key_ext, value_ext, sink_table, row_start):
    row_count = queries.shape[0]
    kv_heads = key_ext.shape[1] // HEAD
    group_size = queries.shape[1] // HEAD // kv_heads
    blocks = row_count // WINDOW
    query_blocks = queries.reshape(blocks, WINDOW, kv_heads, group_size, HEAD)

    def banded(table):
        table = table.reshape(blocks + 1, WINDOW, kv_heads, HEAD)
        return jnp.concatenate([table[:-1], table[1:]], axis=1)

    key_band = banded(key_ext)
    value_band = banded(value_ext)
    scores = jnp.einsum(
        "nqhgd,nkhd->nhgqk", query_blocks, key_band, preferred_element_type=jnp.float32
    ) * HEAD ** (-0.5)
    query_index = jnp.arange(WINDOW, dtype=jnp.int32)[:, None]
    key_index = jnp.arange(2 * WINDOW, dtype=jnp.int32)[None, :]
    offset = query_index + WINDOW - key_index
    key_position = (
        row_start + jnp.arange(blocks, dtype=jnp.int32)[:, None, None] * WINDOW + key_index - WINDOW
    )
    valid_mask = ((offset >= 0) & (offset < WINDOW) & (key_position >= 0))[:, None, None]
    scores = jnp.where(valid_mask, scores, NEGATIVE)
    sink_logit = sink_table.reshape(1, kv_heads, group_size, 1, 1)
    row_top = jnp.maximum(jnp.max(scores, axis=-1, keepdims=True), sink_logit)
    weights = jnp.where(valid_mask, jnp.exp(scores - row_top), 0.0)
    denominator = jnp.sum(weights, axis=-1, keepdims=True) + jnp.exp(sink_logit - row_top)
    probabilities = (weights / denominator).astype(jnp.bfloat16)
    attended = jnp.einsum(
        "nhgqk,nkhd->nqhgd", probabilities, value_band, preferred_element_type=jnp.float32
    )
    return attended.astype(jnp.bfloat16).reshape(row_count, kv_heads * group_size * HEAD)


def on_device(
    features,
    norm_gain,
    w_query,
    w_key,
    w_value,
    head_sinks,
    w_query_latent,
    w_kv_latent,
    w_rope_key,
    query_latent_gain,
    kv_latent_gain,
    w_query_content,
    w_query_rotary,
    w_key_up,
    w_value_up,
    w_branch_window,
    w_branch_latent,
    w_gate_window,
    w_gate_latent,
):
    tok_rows = features.shape[0]
    row_start = lax.axis_index("sp") * tok_rows
    row_end = row_start + tok_rows
    positions = row_start + jnp.arange(tok_rows, dtype=jnp.int32)
    gathered = gathered_copies(features, "tp", 1)
    normed = rms_rows(gathered.astype(jnp.float32), norm_gain).astype(jnp.bfloat16)
    query_rows = project(normed, w_query).astype(jnp.bfloat16)
    key_rows = project(normed, w_key).astype(jnp.bfloat16)
    value_rows = project(normed, w_value).astype(jnp.bfloat16)
    key_width = key_rows.shape[1]
    packed = jnp.concatenate([key_rows, value_rows], axis=1)
    tail_rows = from_behind(packed[tok_rows - WINDOW :], "sp", 1)
    extended = jnp.concatenate([tail_rows, packed], axis=0)
    window_out = window_attention(
        query_rows, extended[:, :key_width], extended[:, key_width:], head_sinks, row_start
    )
    latent_query = rms_rows(project(normed, w_query_latent), query_latent_gain).astype(jnp.bfloat16)
    latent_kv = rms_rows(project(normed, w_kv_latent), kv_latent_gain).astype(jnp.bfloat16)
    rope_rows = rotate(project(normed, w_rope_key), positions).astype(jnp.bfloat16)
    lat_heads = w_key_up.shape[1] // NOPE
    query_content = (
        project(latent_query, w_query_content)
        .astype(jnp.bfloat16)
        .reshape(tok_rows, lat_heads, NOPE)
    )
    query_rotary = rotate(
        project(latent_query, w_query_rotary).reshape(tok_rows, lat_heads, ROPE), positions
    ).astype(jnp.bfloat16)
    scale_factor = (NOPE + ROPE) ** (-0.5)

    def attend(running, piece_keys, piece_values, rope_piece):
        running_max, denominator, accumulated = running
        piece_rows = piece_keys.shape[0]
        scores = (
            jnp.einsum(
                "qhd,khd->hqk",
                query_content,
                piece_keys.reshape(piece_rows, lat_heads, NOPE),
                preferred_element_type=jnp.float32,
            )
            + jnp.einsum(
                "qhr,kr->hqk", query_rotary, rope_piece, preferred_element_type=jnp.float32
            )
        ) * scale_factor
        key_position = jnp.arange(piece_rows, dtype=jnp.int32)
        live_mask = key_position[None, :] <= positions[:, None]
        scores = jnp.where(live_mask, scores, NEGATIVE)
        new_max = jnp.maximum(running_max, jnp.max(scores, axis=-1))
        weights = jnp.where(live_mask, jnp.exp(scores - new_max[..., None]), 0.0)
        denominator = jnp.sum(weights, axis=-1)
        accumulated = jnp.einsum(
            "hqk,khd->hqd",
            weights.astype(jnp.bfloat16),
            piece_values.reshape(piece_rows, lat_heads, VDIM),
            preferred_element_type=jnp.float32,
        )
        return (new_max, denominator, accumulated)

    initial = (
        jnp.full((lat_heads, tok_rows), NEGATIVE, jnp.float32),
        jnp.zeros((lat_heads, tok_rows), jnp.float32),
        jnp.zeros((lat_heads, tok_rows, VDIM), jnp.float32),
    )
    own_keys = project(latent_kv, w_key_up).astype(jnp.bfloat16)
    own_values = project(latent_kv, w_value_up).astype(jnp.bfloat16)
    pieces = in_one_piece((own_keys, own_values, rope_rows), "sp", 0, 1)
    running = lax.cond(
        jnp.int32(0) < row_end,
        lambda current: attend(current, pieces[0], pieces[1], pieces[2]),
        lambda current: current,
        initial,
    )
    latent_out = jnp.transpose(running[2] / running[1][..., None], (1, 0, 2))
    latent_out = latent_out.reshape(tok_rows, lat_heads * VDIM).astype(jnp.bfloat16)
    all_window, all_latent = in_one_piece((window_out, latent_out), "tp", 1, 0)
    column_window, column_latent = (
        lax.all_to_all(w_branch_window, "tp", split_axis=1, concat_axis=0, tiled=True),
        lax.all_to_all(w_branch_latent, "tp", split_axis=1, concat_axis=0, tiled=True),
    )
    window_branch = project(all_window, column_window)
    latent_branch = project(all_latent, column_latent)
    window_gate = jax.nn.sigmoid(project(normed, w_gate_window))
    latent_gate = jax.nn.sigmoid(project(normed, w_gate_latent))
    return (window_gate * window_branch + latent_gate * latent_branch).astype(jnp.bfloat16)


def solution(mesh):
    return jax.shard_map(
        on_device,
        mesh=mesh,
        in_specs=(
            P("sp", "tp"),
            P(),
            P(None, "tp"),
            P(None, "tp"),
            P(None, "tp"),
            P("tp"),
            P(),
            P(),
            P(),
            P(),
            P(),
            P(None, "tp"),
            P(None, "tp"),
            P(None, "tp"),
            P(None, "tp"),
            P("tp", None),
            P("tp", None),
            P(None, "tp"),
            P(None, "tp"),
        ),
        out_specs=P("sp", "tp"),
        check_vma=False,
    )
```

profile of v0, /device:TPU:36, one launch (start us, length us, event | category | flops | bytes accessed | tf_op | source)
XLA Modules:
  0.0 250.7 jit_solution(12856816892344930347)
XLA Ops:
  6.5 1.2 copy.42
  7.8 1.3 broadcast_in_dim.36
  9.1 4.5 %all-to-all-start = ((bf16[8,384,256]{1,2,0:T(8,128)(2,1)}), bf16[8,384,256]{1,2,0:T(8,128)(2,1)}, u32[]{:S(2)}, u32[]{:S(2)}) async-start(bf16[8,384,256]{1,2,0:T(8,128)(2,1)} %broadcast_in_dim.36), calls=%async_computation | async-start | bytes 3145728 | tf_op jit(solution)/shard_map/all_to_all | solution.py:18
  13.6 21.6 %all-to-all-done = bf16[8,384,256]{1,2,0:T(8,128)(2,1)} async-done(((bf16[8,384,256]{1,2,0:T(8,128)(2,1)}), bf16[8,384,256]{1,2,0:T(8,128)(2,1)}, u32[]{:S(2)}, u32[]{:S(2)}) %all-to-all-start) | async-done | bytes 1572896 | tf_op jit(solution)/shard_map/all_to_all | solution.py:18
  35.2 1.8 multiply_reduce_fusion
  37.0 1.8 fusion.19
  38.9 1.1 multiply_reduce_fusion.2
  41.5 0.7 pad_maximum_fusion
  42.6 1.9 convolution_convert_fusion.5
  44.6 1.8 convolution_convert_fusion.6
  46.4 3.2 %collective-permute-start = (bf16[128,128]{0,1:T(8,128)(2,1)S(1)}, bf16[128,128]{0,1:T(8,128)(2,1)S(1)}, u32[]{:S(2)}, u32[]{:S(2)}) collective-permute-start(bf16[128,128]{0,1:T(8,128)(2,1)S(1)} %pad_maximum_fusion.6), channel_id=1, source_target_pairs={{0,8},{8,16},{16,24},{24,32},{32,40},{40,48},{48,56},{56,64},{64,7... | collective-permute-start | bytes 98312 | tf_op jit(solution)/shard_map/ppermute | solution.py:37
  49.7 1.1 multiply_reduce_fusion.1
  51.8 0.6 convolution_convert_fusion.4
  53.8 89.5 %all-gather.3.cloned.1.call-done = bf16[12288,320]{0,1:T(8,128)(2,1)} async-done(((bf16[384,320]{0,1:T(8,128)(2,1)}), bf16[12288,320]{0,1:T(8,128)(2,1)}) %all-gather.3.cloned.1.call-update) | async-done | bytes 7864336 | tf_op jit(solution)/shard_map/all_gather | solution.py:43
  143.3 59.5 %conditional.1 = (f32[1,384]{1,0:T(1,128)S(1)}, f32[1,384,128]{1,2,0:T(8,128)S(1)}) conditional(s32[]{:T(128)} %convert_element_type.97, () %tuple.13, (s32[]{:T(128)}, s32[384]{0:T(512)S(1)}, bf16[12288,320]{0,1:T(8,128)(2,1)}, bf16[384,128]{1,0:T(8,128)(2,1)S(1)}, bf16[384,1,64]{0,2,1:T(8,128)(2,1)S(1)}) %tuple.14), branch_computations={%region_5.6_spmd, %region_6.9_spmd} | conditional | flops 3081240576 | bytes 119901712 | solution.py:199
  143.3 11.6 %copy.51 = bf16[12288,320]{1,0:T(8,128)(2,1)} copy(bf16[12288,320]{0,1:T(8,128)(2,1)} %get-tuple-element.44) | data formatting | bytes 15728640 | tf_op jit(solution)/shard_map
  154.9 9.8 %fusion.9 = f32[384,12288]{1,0:T(8,128)} fusion(bf16[384,128]{1,0:T(8,128)(2,1)S(1)} %get-tuple-element.25, bf16[12288,320]{1,0:T(8,128)(2,1)} %copy.51), kind=kOutput, calls=%fused_computation.11 | convolution fusion | flops 1207959552 | bytes 22118400 | tf_op jit(solution)/shard_map/cond/branch_1_fun/qhd,khd->hqk/dot_general | solution.py:167
  164.7 16.8 %fusion.63 = (f32[384]{0:T(512)S(1)}, f32[1,384,12288]{2,1,0:T(8,128)}) fusion(bf16[384,1,64]{0,2,1:T(8,128)(2,1)S(1)} %get-tuple-element.27, bf16[12288,320]{1,0:T(8,128)(2,1)} %copy.51, f32[384,12288]{1,0:T(8,128)} %fusion.9, s32[384]{0:T(512)S(1)} %broadcast_add_fusion), kind=kOutput, calls=%fused_computation.111 | convolution fusion | flops 627572352 | bytes 40946688 | tf_op jit(solution)/shard_map/cond/branch_1_fun/qhr,kr->hqk/dot_general | solution.py:173
  181.5 10.2 %fusion.11 = f32[1,384,128]{1,2,0:T(8,128)S(1)} fusion(bf16[12288,320]{1,0:T(8,128)(2,1)} %copy.51, f32[1,384,12288]{2,1,0:T(8,128)} %get-tuple-element.49, f32[384]{0:T(512)S(1)} %broadcast_maximum_fusion, s32[384]{0:T(512)S(1)} %broadcast_add_fusion), kind=kOutput, calls=%fused_computation.13 | convolution fusion | flops 1226833920 | bytes 22219776 | tf_op jit(solution)/shard_map/cond/branch_1_fun/hqk,khd->hqd/dot_general | solution.py:183
  191.7 11.1 %fusion.3 = f32[384]{0:T(512)S(1)} fusion(f32[1,384,12288]{2,1,0:T(8,128)} %get-tuple-element.49, f32[384]{0:T(512)S(1)} %broadcast_maximum_fusion, s32[384]{0:T(512)S(1)} %broadcast_add_fusion), kind=kLoop, calls=%fused_computation.6 | loop fusion | flops 18873984 | bytes 18878976 | tf_op jit(solution)/shard_map/cond/branch_1_fun/reduce_sum | solution.py:182
  202.9 0.7 pad_maximum_fusion.1
  203.6 1.0 copy.55
  204.6 4.3 %all-to-all-start.2 = ((bf16[128,8,256]{0,2,1:T(8,128)(2,1)}), bf16[128,8,256]{0,2,1:T(8,128)(2,1)S(1)}, u32[]{:S(2)}, u32[]{:S(2)}) async-start(bf16[128,8,256]{0,2,1:T(8,128)(2,1)} %bitcast.24), calls=%async_computation.2 | async-start | bytes 1048576 | tf_op jit(solution)/shard_map/all_to_all | solution.py:210
  208.9 1.0 copy.53
  209.9 10.4 %all-to-all-done.2 = bf16[128,8,256]{0,2,1:T(8,128)(2,1)S(1)} async-done(((bf16[128,8,256]{0,2,1:T(8,128)(2,1)}), bf16[128,8,256]{0,2,1:T(8,128)(2,1)S(1)}, u32[]{:S(2)}, u32[]{:S(2)}) %all-to-all-start.2) | async-done | bytes 524320 | tf_op jit(solution)/shard_map/all_to_all | solution.py:210
  220.3 3.7 %all-to-all-start.1 = ((bf16[128,8,256]{0,2,1:T(8,128)(2,1)}), bf16[128,8,256]{0,2,1:T(8,128)(2,1)S(1)}, u32[]{:S(2)}, u32[]{:S(2)}) async-start(bf16[128,8,256]{0,2,1:T(8,128)(2,1)} %bitcast.21), calls=%async_computation.1 | async-start | bytes 1048576 | tf_op jit(solution)/shard_map/all_to_all | solution.py:209
  224.2 9.8 %all-to-all-done.1 = bf16[128,8,256]{0,2,1:T(8,128)(2,1)S(1)} async-done(((bf16[128,8,256]{0,2,1:T(8,128)(2,1)}), bf16[128,8,256]{0,2,1:T(8,128)(2,1)S(1)}, u32[]{:S(2)}, u32[]{:S(2)}) %all-to-all-start.1) | async-done | bytes 524320 | tf_op jit(solution)/shard_map/all_to_all | solution.py:209
  234.0 1.0 copy.54
  235.1 2.7 %fusion.28 = f32[384,256]{1,0:T(8,128)} fusion(bf16[384,2048]{0,1:T(8,128)(2,1)S(1)} %copy-done.3, bf16[2048,256]{1,0:T(8,128)(2,1)} %param.39), kind=kOutput, calls=%fused_computation.35 | convolution fusion | flops 402948096 | bytes 3014656 | tf_op jit(solution)/shard_map/dot_general | solution.py:74
  237.8 2.2 fusion.25
  240.0 1.6 convolution_multiply_fusion.1
  241.6 2.2 fusion.29
  (91 shorter events, 4.5 us)
Async XLA Ops:
  6.5 32.3 %copy-start = (bf16[2048,512]{1,0:T(8,128)(2,1)S(1)}, bf16[2048,512]{1,0:T(8,128)(2,1)}, u32[]{:S(2)}) copy-start(bf16[2048,512]{1,0:T(8,128)(2,1)} %param.28) | copy-start | bytes 6291460
  7.8 29.2 %copy-start.15 = (f32[2048]{0:T(1024)S(1)}, f32[2048]{0:T(1024)}, u32[]{:S(2)}) copy-start(f32[2048]{0:T(1024)} %param.22) | copy-start | bytes 24580
  9.1 26.1 %all-to-all-start = ((bf16[8,384,256]{1,2,0:T(8,128)(2,1)}), bf16[8,384,256]{1,2,0:T(8,128)(2,1)}, u32[]{:S(2)}, u32[]{:S(2)}) async-start(bf16[8,384,256]{1,2,0:T(8,128)(2,1)} %broadcast_in_dim.36), calls=%async_computation | async-start | bytes 3145728 | tf_op jit(solution)/shard_map/all_to_all | solution.py:18
  13.5 129.8 %all-gather.3.cloned.1.call-start = ((), (), s32[]{:S(2)}) async-start(), calls=%async_computation.3 | async-start | bytes 8110080 | tf_op jit(solution)/shard_map/all_gather | solution.py:43
  38.9 2.0 copy-start.2
  38.9 1.2 copy-start.11
  38.9 1.2 copy-start.16
  38.9 1.5 copy-start.12
  38.9 1.9 copy-start.10
  40.0 2.6 %copy-start.8 = (bf16[2048,64]{0,1:T(8,128)(2,1)S(1)}, bf16[2048,64]{0,1:T(8,128)(2,1)}, u32[]{:S(2)}) copy-start(bf16[2048,64]{0,1:T(8,128)(2,1)} %param.25) | copy-start | bytes 786436
  40.4 4.1 %copy-start.9 = (bf16[2048,64]{0,1:T(8,128)(2,1)S(1)}, bf16[2048,64]{0,1:T(8,128)(2,1)}, u32[]{:S(2)}) copy-start(bf16[2048,64]{0,1:T(8,128)(2,1)} %param.24) | copy-start | bytes 786436
  41.2 8.4 %copy-start.3 = (bf16[384,2048]{0,1:T(8,128)(2,1)S(1)}, bf16[384,2048]{0,1:T(8,128)(2,1)}, u32[]{:S(2)}) copy-start(bf16[384,2048]{0,1:T(8,128)(2,1)} %copy-done.2) | copy-start | bytes 4718596
  42.3 197.7 %all-gather.5.cloned.1.call-start = ((), (), s32[]{:S(2)}) async-start(), calls=%async_computation.4 | async-start | bytes 1769472 | tf_op jit(solution)/shard_map/all_gather | solution.py:43
  42.3 7.4 %copy-start.19 = (bf16[2048,512]{1,0:T(8,128)(2,1)S(1)}, bf16[2048,512]{1,0:T(8,128)(2,1)}, u32[]{:S(2)}) copy-start(bf16[2048,512]{1,0:T(8,128)(2,1)} %param.27) | copy-start | bytes 6291460
  46.4 4.4 %copy-start.14 = (bf16[512,64]{0,1:T(8,128)(2,1)S(1)}, bf16[512,64]{0,1:T(8,128)(2,1)}, u32[]{:S(2)}) copy-start(bf16[512,64]{0,1:T(8,128)(2,1)} %param.33) | copy-start | bytes 196612
  46.4 4.4 %copy-start.17 = (f32[512]{0:T(512)S(1)}, f32[512]{0:T(512)}, u32[]{:S(2)}) copy-start(f32[512]{0:T(512)} %param.30) | copy-start | bytes 6148
  46.4 5.0 %copy-start.13 = (bf16[512,128]{1,0:T(8,128)(2,1)S(1)}, bf16[512,128]{1,0:T(8,128)(2,1)}, u32[]{:S(2)}) copy-start(bf16[512,128]{1,0:T(8,128)(2,1)} %param.32) | copy-start | bytes 393220
  46.4 5.4 %copy-start.7 = (bf16[2048,128]{1,0:T(8,128)(2,1)S(1)}, bf16[2048,128]{1,0:T(8,128)(2,1)}, u32[]{:S(2)}) copy-start(bf16[2048,128]{1,0:T(8,128)(2,1)} %param.23) | copy-start | bytes 1572868
  46.4 6.2 %collective-permute-start = (bf16[128,128]{0,1:T(8,128)(2,1)S(1)}, bf16[128,128]{0,1:T(8,128)(2,1)S(1)}, u32[]{:S(2)}, u32[]{:S(2)}) collective-permute-start(bf16[128,128]{0,1:T(8,128)(2,1)S(1)} %pad_maximum_fusion.6), channel_id=1, source_target_pairs={{0,8},{8,16},{16,24},{24,32},{32,40},{40,48},{48,56},{56,64},{64,7... | collective-permute-start | bytes 98312 | tf_op jit(solution)/shard_map/ppermute | solution.py:37
  51.4 1.6 copy-start.18
  143.3 60.3 %copy-start.4 = (bf16[128,2048]{1,0:T(8,128)(2,1)S(1)}, bf16[128,2048]{1,0:T(8,128)(2,1)}, u32[]{:S(2)}) copy-start(bf16[128,2048]{1,0:T(8,128)(2,1)} %param.37) | copy-start | bytes 1572868
  202.8 6.1 %copy-start.5 = (bf16[128,2048]{1,0:T(8,128)(2,1)S(1)}, bf16[128,2048]{1,0:T(8,128)(2,1)}, u32[]{:S(2)}) copy-start(bf16[128,2048]{1,0:T(8,128)(2,1)} %param.36) | copy-start | bytes 1572868
  204.6 15.7 %all-to-all-start.2 = ((bf16[128,8,256]{0,2,1:T(8,128)(2,1)}), bf16[128,8,256]{0,2,1:T(8,128)(2,1)S(1)}, u32[]{:S(2)}, u32[]{:S(2)}) async-start(bf16[128,8,256]{0,2,1:T(8,128)(2,1)} %bitcast.24), calls=%async_computation.2 | async-start | bytes 1048576 | tf_op jit(solution)/shard_map/all_to_all | solution.py:210
  220.3 13.7 %all-to-all-start.1 = ((bf16[128,8,256]{0,2,1:T(8,128)(2,1)}), bf16[128,8,256]{0,2,1:T(8,128)(2,1)S(1)}, u32[]{:S(2)}, u32[]{:S(2)}) async-start(bf16[128,8,256]{0,2,1:T(8,128)(2,1)} %bitcast.21), calls=%async_computation.1 | async-start | bytes 1048576 | tf_op jit(solution)/shard_map/all_to_all | solution.py:209
  235.1 2.7 %copy-start.20 = (bf16[2048,256]{1,0:T(8,128)(2,1)S(1)}, bf16[2048,256]{1,0:T(8,128)(2,1)}, u32[]{:S(2)}) copy-start(bf16[2048,256]{1,0:T(8,128)(2,1)} %param.38) | copy-start | bytes 3145732
  237.8 3.9 %copy-start.6 = (bf16[8,128,256]{2,1,0:T(8,128)(2,1)S(1)}, bf16[8,128,256]{2,1,0:T(8,128)(2,1)}, u32[]{:S(2)}) copy-start(bf16[8,128,256]{2,1,0:T(8,128)(2,1)} %copy.54) | copy-start | bytes 1572868
  237.8 6.1 %copy-start.1 = (bf16[2048,512]{1,0:T(8,128)(2,1)S(1)}, bf16[2048,512]{1,0:T(8,128)(2,1)}, u32[]{:S(2)}) copy-start(bf16[2048,512]{1,0:T(8,128)(2,1)} %param.28) | copy-start | bytes 6291460
Sparse Core Ops, SparseCore 0:
  42.4 100.8 all-gather.2
  203.7 27.3 all-gather.4
where the time goes:
time: 252 us; the launch traced here: 251 us
  waiting for transfers between devices  131 us (52%)
  matrix products  54.4 us (22%)
  local copies, waits for them, and re-layouts  17.9 us (7%)
  other arithmetic  17.4 us (7%)
  starting transfers between devices  15.8 us (6%)
  between operations  14 us (6%)
    all_gather x2, waiting for transfers between devices, in_one_piece(): result = lax.all_gather(both, axis, axis=dim, tiled=True)  89.5 us
    all_to_all x1, waiting for transfers between devices, copy_for_each(): lax.all_to_all(jnp.broadcast_to(shard[None], (count, *shard.shape)), axis...  21.6 us
    dot_general x14, matrix products, project(): return jnp.dot(left, right, preferred_element_type=jnp.float32)  17 us
    dot_general x1, matrix products, attend(): jnp.einsum('qhr,kr->hqk', query_rotary, rope_piece, preferred_element_typ...  16.8 us
    another operation x2, local copies, waits for them, and re-layouts  11.7 us
    reduce_sum x1, other arithmetic, attend(): denominator = jnp.sum(weights, axis=-1)  11.1 us
    all_to_all x1, waiting for transfers between devices, on_device(): lax.all_to_all(w_branch_latent, 'tp', split_axis=1, concat_axis=0, tiled=...  10.4 us
    dot_general x1, matrix products, attend(): jnp.einsum('hqk,khd->hqd', weights.astype(jnp.bfloat16), piece_values.res...  10.2 us
  transfers between devices with their start and end apart: 6, of which 4 were waited for; matrix products, arithmetic and copies ran while one was open for 6% of the time, Pallas kernels for 0%

commit v1 on v0

--- a/solution.py
+++ b/solution.py
@@ -11,6 +11,29 @@
 EPS = 1e-06
 THETA = 10000.0
 NEGATIVE = -1e30
+
+
+def in_blocks(array, dim, peers):
+    dims = array.shape
+    blocks = array.reshape(*dims[:dim], peers, dims[dim] // peers, *dims[dim + 1 :])
+    return jnp.moveaxis(blocks, dim, 0)
+
+
+def in_order_2(pieces, dim):
+    pieces = jnp.moveaxis(pieces, 0, dim)
+    lengths = pieces.shape
+    return pieces.reshape(*lengths[:dim], lengths[dim] * lengths[dim + 1], *lengths[dim + 2 :])
+
+
+def exchange_in_pairs(x, axis, split_dim, concat_dim):
+    devices, mine = (lax.axis_size(axis), lax.axis_index(axis))
+    parts = in_blocks(x, split_dim, devices)
+    finished = [parts[mine]]
+    for hop in range(1, devices):
+        sent = parts[mine ^ hop]
+        finished.append(lax.ppermute(sent, axis, [(i, i ^ hop) for i in range(devices)]))
+    parts = jnp.stack(finished)[mine ^ jnp.arange(devices)]
+    return in_order_2(parts, concat_dim)
 
 
 def copy_for_each(shard, axis):
@@ -207,7 +230,7 @@
     all_window, all_latent = in_one_piece((window_out, latent_out), "tp", 1, 0)
     column_window, column_latent = (
         lax.all_to_all(w_branch_window, "tp", split_axis=1, concat_axis=0, tiled=True),
-        lax.all_to_all(w_branch_latent, "tp", split_axis=1, concat_axis=0, tiled=True),
+        exchange_in_pairs(w_branch_latent, "tp", 1, 0),
     )
     window_branch = project(all_window, column_window)
     latent_branch = project(all_latent, column_latent)

time: 252 us -> 243 us (0.964)
  waiting for transfers between devices: 131 us -> 119 us
  starting transfers between devices: 15.8 us -> 20.2 us
    all_to_all x1 -> x0, waiting for transfers between devices: 10.4 us -> none  [on_device(): lax.all_to_all(w_branch_latent, 'tp', split_axis=1, concat_axis=0, tiled=...]
    all_to_all x1, waiting for transfers between devices: 9.8 us -> 0.01 us  [on_device(): lax.all_to_all(w_branch_window, 'tp', split_axis=1, concat_axis=0, tiled=...]
    ppermute x0 -> x7, starting transfers between devices: none -> 8.89 us  [exchange_in_pairs(): lax.ppermute(sent, axis, [(i, i ^ hop) for i in range(devices)])]
    ppermute x0 -> x7, waiting for transfers between devices: none -> 4.84 us  [exchange_in_pairs(): lax.ppermute(sent, axis, [(i, i ^ hop) for i in range(devices)])]
    all_to_all x1 -> x0, starting transfers between devices: 4.29 us -> none  [on_device(): lax.all_to_all(w_branch_latent, 'tp', split_axis=1, concat_axis=0, tiled=...]
    all_gather x2, waiting for transfers between devices: 89.5 us -> 92.2 us  [in_one_piece(): result = lax.all_gather(both, axis, axis=dim, tiled=True)]
    another operation x2 -> x12, local copies, waits for them, and re-layouts: 11.7 us -> 12.6 us
  transfers between devices with their start and end apart: 6 -> 12, of which waited for: 4 -> 6; matrix products, arithmetic and copies ran while one was open for 6% -> 31% of each run, Pallas kernels for 0% -> 0%
where the time goes in v1:
time: 243 us; the launch traced here: 240 us
  waiting for transfers between devices  119 us (49%)
  matrix products  52.3 us (22%)
  starting transfers between devices  20.2 us (8%)
  local copies, waits for them, and re-layouts  17.6 us (7%)
  other arithmetic  17.4 us (7%)
  between operations  14.2 us (6%)
    all_gather x2, waiting for transfers between devices, in_one_piece(): result = lax.all_gather(both, axis, axis=dim, tiled=True)  92.2 us
    all_to_all x1, waiting for transfers between devices, copy_for_each(): lax.all_to_all(jnp.broadcast_to(shard[None], (count, *shard.shape)), axis...  21.6 us
    dot_general x1, matrix products, attend(): jnp.einsum('qhr,kr->hqk', query_rotary, rope_piece, preferred_element_typ...  16.7 us
    dot_general x14, matrix products, project(): return jnp.dot(left, right, preferred_element_type=jnp.float32)  15 us
    another operation x11, local copies, waits for them, and re-layouts  12.6 us
    reduce_sum x1, other arithmetic, attend(): denominator = jnp.sum(weights, axis=-1)  11.1 us
    dot_general x1, matrix products, attend(): jnp.einsum('hqk,khd->hqd', weights.astype(jnp.bfloat16), piece_values.res...  10.2 us
    dot_general x1, matrix products, attend(): jnp.einsum('qhd,khd->hqk', query_content, piece_keys.reshape(piece_rows,...  9.75 us
  transfers between devices with their start and end apart: 12, of which 6 were waited for; matrix products, arithmetic and copies ran while one was open for 31% of the time, Pallas kernels for 0%

profile of v1, /device:TPU:36, one launch (start us, length us, event | category | flops | bytes accessed | tf_op | source)
XLA Modules:
  0.0 240.3 jit_solution(14132055040269838728)
XLA Ops:
  6.5 1.2 copy.42
  7.8 1.3 broadcast_in_dim.36
  9.1 4.5 %all-to-all-start = ((bf16[8,384,256]{1,2,0:T(8,128)(2,1)}), bf16[8,384,256]{1,2,0:T(8,128)(2,1)}, u32[]{:S(2)}, u32[]{:S(2)}) async-start(bf16[8,384,256]{1,2,0:T(8,128)(2,1)} %broadcast_in_dim.36), calls=%async_computation | async-start | bytes 3145728 | tf_op jit(solution)/shard_map/all_to_all | solution.py:41
  13.6 21.6 %all-to-all-done = bf16[8,384,256]{1,2,0:T(8,128)(2,1)} async-done(((bf16[8,384,256]{1,2,0:T(8,128)(2,1)}), bf16[8,384,256]{1,2,0:T(8,128)(2,1)}, u32[]{:S(2)}, u32[]{:S(2)}) %all-to-all-start) | async-done | bytes 1572896 | tf_op jit(solution)/shard_map/all_to_all | solution.py:41
  35.2 1.8 multiply_reduce_fusion
  37.0 1.8 fusion.19
  39.3 1.1 multiply_reduce_fusion.2
  41.5 0.7 pad_maximum_fusion
  42.3 1.0 copy.53
  43.3 3.5 %all-to-all-start.1 = ((bf16[128,8,256]{0,2,1:T(8,128)(2,1)}), bf16[128,8,256]{0,2,1:T(8,128)(2,1)S(1)}, u32[]{:S(2)}, u32[]{:S(2)}) async-start(bf16[128,8,256]{0,2,1:T(8,128)(2,1)} %bitcast.21), calls=%async_computation.1 | async-start | bytes 1048576 | tf_op jit(solution)/shard_map/all_to_all | solution.py:232
  47.9 1.3 convolution_convert_fusion.5
  49.3 3.2 %collective-permute-start = (bf16[128,128]{0,1:T(8,128)(2,1)S(1)}, bf16[128,128]{0,1:T(8,128)(2,1)S(1)}, u32[]{:S(2)}, u32[]{:S(2)}) collective-permute-start(bf16[128,128]{0,1:T(8,128)(2,1)S(1)} %pad_maximum_fusion.6), channel_id=1, source_target_pairs={{0,8},{8,16},{16,24},{24,32},{32,40},{40,48},{48,56},{56,64},{64,7... | collective-permute-start | bytes 98312 | tf_op jit(solution)/shard_map/ppermute | solution.py:60
  52.5 1.1 multiply_reduce_fusion.1
  56.7 86.6 %all-gather.3.cloned.1.call-done = bf16[12288,320]{0,1:T(8,128)(2,1)} async-done(((bf16[384,320]{0,1:T(8,128)(2,1)}), bf16[12288,320]{0,1:T(8,128)(2,1)}) %all-gather.3.cloned.1.call-update) | async-done | bytes 7864336 | tf_op jit(solution)/shard_map/all_gather | solution.py:66
  143.3 59.4 %conditional.1 = (f32[1,384]{1,0:T(1,128)S(1)}, f32[1,384,128]{1,2,0:T(8,128)S(1)}) conditional(s32[]{:T(128)} %convert_element_type.97, () %tuple.13, (s32[]{:T(128)}, s32[384]{0:T(512)S(1)}, bf16[12288,320]{0,1:T(8,128)(2,1)}, bf16[384,128]{1,0:T(8,128)(2,1)S(1)}, bf16[384,1,64]{0,2,1:T(8,128)(2,1)S(1)}) %tuple.14), branch_computations={%region_5.6_spmd, %region_6.9_spmd} | conditional | flops 3081240576 | bytes 119901712 | solution.py:222
  143.3 11.6 %copy.51 = bf16[12288,320]{1,0:T(8,128)(2,1)} copy(bf16[12288,320]{0,1:T(8,128)(2,1)} %get-tuple-element.44) | data formatting | bytes 15728640 | tf_op jit(solution)/shard_map
  154.9 9.7 %fusion.9 = f32[384,12288]{1,0:T(8,128)} fusion(bf16[384,128]{1,0:T(8,128)(2,1)S(1)} %get-tuple-element.25, bf16[12288,320]{1,0:T(8,128)(2,1)} %copy.51), kind=kOutput, calls=%fused_computation.12 | convolution fusion | flops 1207959552 | bytes 22118400 | tf_op jit(solution)/shard_map/cond/branch_1_fun/qhd,khd->hqk/dot_general | solution.py:190
  164.7 16.7 %fusion.64 = (f32[384]{0:T(512)S(1)}, f32[1,384,12288]{2,1,0:T(8,128)}) fusion(bf16[384,1,64]{0,2,1:T(8,128)(2,1)S(1)} %get-tuple-element.27, bf16[12288,320]{1,0:T(8,128)(2,1)} %copy.51, f32[384,12288]{1,0:T(8,128)} %fusion.9, s32[384]{0:T(512)S(1)} %broadcast_add_fusion), kind=kOutput, calls=%fused_computation.131 | convolution fusion | flops 627572352 | bytes 40946688 | tf_op jit(solution)/shard_map/cond/branch_1_fun/qhr,kr->hqk/dot_general | solution.py:196
  181.3 10.2 %fusion.11 = f32[1,384,128]{1,2,0:T(8,128)S(1)} fusion(bf16[12288,320]{1,0:T(8,128)(2,1)} %copy.51, f32[1,384,12288]{2,1,0:T(8,128)} %get-tuple-element.49, f32[384]{0:T(512)S(1)} %broadcast_maximum_fusion, s32[384]{0:T(512)S(1)} %broadcast_add_fusion), kind=kOutput, calls=%fused_computation.14 | convolution fusion | flops 1226833920 | bytes 22219776 | tf_op jit(solution)/shard_map/cond/branch_1_fun/hqk,khd->hqd/dot_general | solution.py:206
  191.6 11.1 %fusion.3 = f32[384]{0:T(512)S(1)} fusion(f32[1,384,12288]{2,1,0:T(8,128)} %get-tuple-element.49, f32[384]{0:T(512)S(1)} %broadcast_maximum_fusion, s32[384]{0:T(512)S(1)} %broadcast_add_fusion), kind=kLoop, calls=%fused_computation.7 | loop fusion | flops 18873984 | bytes 18878976 | tf_op jit(solution)/shard_map/cond/branch_1_fun/reduce_sum | solution.py:205
  202.7 0.7 pad_maximum_fusion.1
  203.8 1.6 collective-permute-start.2
  206.1 3.3 %collective-permute-start.4 = (bf16[128,256]{1,0:T(8,128)(2,1)S(1)}, bf16[128,256]{1,0:T(8,128)(2,1)S(1)}, u32[]{:S(2)}, u32[]{:S(2)}) collective-permute-start(bf16[128,256]{1,0:T(8,128)(2,1)S(1)} %bitcast.138), channel_id=1, source_target_pairs={{0,4},{1,5},{2,6},{3,7},{4,0},{5,1},{6,2},{7,3},{8,12},{9,13},{10,... | collective-permute-start | bytes 196616 | tf_op jit(solution)/shard_map/ppermute | solution.py:34
  210.1 2.8 %collective-permute-start.6 = (bf16[128,256]{1,0:T(8,128)(2,1)S(1)}, bf16[128,256]{1,0:T(8,128)(2,1)S(1)}, u32[]{:S(2)}, u32[]{:S(2)}) collective-permute-start(bf16[128,256]{1,0:T(8,128)(2,1)S(1)} %bitcast.139), channel_id=1, source_target_pairs={{0,6},{1,7},{2,4},{3,5},{4,2},{5,3},{6,0},{7,1},{8,14},{9,15},{10,... | collective-permute-start | bytes 196616 | tf_op jit(solution)/shard_map/ppermute | solution.py:34
  213.4 2.0 collective-permute-done.5
  215.4 1.5 collective-permute-done.6
  216.9 1.4 collective-permute-done.7
  219.1 1.9 fusion.27
  221.1 3.0 %fusion.25 = f32[384,256]{1,0:T(8,128)} fusion(bf16[384,2048]{0,1:T(8,128)(2,1)} %copy-done.2, bf16[2048,256]{1,0:T(8,128)(2,1)S(1)} %copy-done.18), kind=kOutput, calls=%fused_computation.33 | convolution fusion | flops 402948096 | bytes 3014656 | tf_op jit(solution)/shard_map/dot_general | solution.py:97
  224.1 5.5 %all-gather.5.cloned.1.call-done = bf16[768,1024]{0,1:T(8,128)(2,1)} async-done(((bf16[768,128]{0,1:T(8,128)(2,1)}), bf16[768,1024]{0,1:T(8,128)(2,1)}) %all-gather.5.cloned.1.call-update) | async-done | bytes 1572880 | tf_op jit(solution)/shard_map/all_gather | solution.py:66
  229.6 1.6 convolution_multiply_fusion.2
  231.2 2.2 fusion.29
  (118 shorter events, 8.4 us)
Async XLA Ops:
  6.5 32.7 %copy-start = (bf16[2048,512]{1,0:T(8,128)(2,1)S(1)}, bf16[2048,512]{1,0:T(8,128)(2,1)}, u32[]{:S(2)}) copy-start(bf16[2048,512]{1,0:T(8,128)(2,1)} %param.28) | copy-start | bytes 6291460
  7.8 29.2 %copy-start.13 = (f32[2048]{0:T(1024)S(1)}, f32[2048]{0:T(1024)}, u32[]{:S(2)}) copy-start(f32[2048]{0:T(1024)} %param.22) | copy-start | bytes 24580
  9.1 26.1 %all-to-all-start = ((bf16[8,384,256]{1,2,0:T(8,128)(2,1)}), bf16[8,384,256]{1,2,0:T(8,128)(2,1)}, u32[]{:S(2)}, u32[]{:S(2)}) async-start(bf16[8,384,256]{1,2,0:T(8,128)(2,1)} %broadcast_in_dim.36), calls=%async_computation | async-start | bytes 3145728 | tf_op jit(solution)/shard_map/all_to_all | solution.py:41
  13.5 25.3 %copy-start.8 = (bf16[2048,64]{0,1:T(8,128)(2,1)S(1)}, bf16[2048,64]{0,1:T(8,128)(2,1)}, u32[]{:S(2)}) copy-start(bf16[2048,64]{0,1:T(8,128)(2,1)} %param.29) | copy-start | bytes 786436
  13.5 129.8 %all-gather.3.cloned.1.call-start = ((), (), s32[]{:S(2)}) async-start(), calls=%async_computation.2 | async-start | bytes 8110080 | tf_op jit(solution)/shard_map/all_gather | solution.py:66
  38.9 1.5 copy-start.2
  39.3 1.2 copy-start.9
  39.3 1.2 copy-start.14
  39.3 1.6 copy-start.10
  39.3 3.0 %copy-start.4 = (bf16[128,2048]{1,0:T(8,128)(2,1)S(1)}, bf16[128,2048]{1,0:T(8,128)(2,1)}, u32[]{:S(2)}) copy-start(bf16[128,2048]{1,0:T(8,128)(2,1)} %param.36) | copy-start | bytes 1572868
  40.4 6.5 %copy-start.5 = (bf16[128,2048]{1,0:T(8,128)(2,1)S(1)}, bf16[128,2048]{1,0:T(8,128)(2,1)}, u32[]{:S(2)}) copy-start(bf16[128,2048]{1,0:T(8,128)(2,1)} %param.37) | copy-start | bytes 1572868
  40.4 7.1 %copy-start.3 = (bf16[384,2048]{0,1:T(8,128)(2,1)S(1)}, bf16[384,2048]{0,1:T(8,128)(2,1)}, u32[]{:S(2)}) copy-start(bf16[384,2048]{0,1:T(8,128)(2,1)} %copy-done.2) | copy-start | bytes 4718596
  40.5 7.1 %copy-start.7 = (bf16[2048,64]{0,1:T(8,128)(2,1)S(1)}, bf16[2048,64]{0,1:T(8,128)(2,1)}, u32[]{:S(2)}) copy-start(bf16[2048,64]{0,1:T(8,128)(2,1)} %param.24) | copy-start | bytes 786436
  43.3 175.6 %all-to-all-start.1 = ((bf16[128,8,256]{0,2,1:T(8,128)(2,1)}), bf16[128,8,256]{0,2,1:T(8,128)(2,1)S(1)}, u32[]{:S(2)}, u32[]{:S(2)}) async-start(bf16[128,8,256]{0,2,1:T(8,128)(2,1)} %bitcast.21), calls=%async_computation.1 | async-start | bytes 1048576 | tf_op jit(solution)/shard_map/all_to_all | solution.py:232
  46.8 182.8 %all-gather.5.cloned.1.call-start = ((), (), s32[]{:S(2)}) async-start(), calls=%async_computation.3 | async-start | bytes 1769472 | tf_op jit(solution)/shard_map/all_gather | solution.py:66
  47.2 5.3 %copy-start.17 = (bf16[2048,512]{1,0:T(8,128)(2,1)S(1)}, bf16[2048,512]{1,0:T(8,128)(2,1)}, u32[]{:S(2)}) copy-start(bf16[2048,512]{1,0:T(8,128)(2,1)} %param.27) | copy-start | bytes 6291460
  49.2 4.4 %copy-start.12 = (bf16[512,64]{0,1:T(8,128)(2,1)S(1)}, bf16[512,64]{0,1:T(8,128)(2,1)}, u32[]{:S(2)}) copy-start(bf16[512,64]{0,1:T(8,128)(2,1)} %param.33) | copy-start | bytes 196612
  49.2 4.4 %copy-start.15 = (f32[512]{0:T(512)S(1)}, f32[512]{0:T(512)}, u32[]{:S(2)}) copy-start(f32[512]{0:T(512)} %param.30) | copy-start | bytes 6148
  49.2 5.0 %copy-start.11 = (bf16[512,128]{1,0:T(8,128)(2,1)S(1)}, bf16[512,128]{1,0:T(8,128)(2,1)}, u32[]{:S(2)}) copy-start(bf16[512,128]{1,0:T(8,128)(2,1)} %param.32) | copy-start | bytes 393220
  49.2 5.4 %copy-start.6 = (bf16[2048,128]{1,0:T(8,128)(2,1)S(1)}, bf16[2048,128]{1,0:T(8,128)(2,1)}, u32[]{:S(2)}) copy-start(bf16[2048,128]{1,0:T(8,128)(2,1)} %param.23) | copy-start | bytes 1572868
  49.3 6.2 %collective-permute-start = (bf16[128,128]{0,1:T(8,128)(2,1)S(1)}, bf16[128,128]{0,1:T(8,128)(2,1)S(1)}, u32[]{:S(2)}, u32[]{:S(2)}) collective-permute-start(bf16[128,128]{0,1:T(8,128)(2,1)S(1)} %pad_maximum_fusion.6), channel_id=1, source_target_pairs={{0,8},{8,16},{16,24},{24,32},{32,40},{40,48},{48,56},{56,64},{64,7... | collective-permute-start | bytes 98312 | tf_op jit(solution)/shard_map/ppermute | solution.py:60
  54.3 1.6 copy-start.16
  203.6 6.5 %collective-permute-start.1 = (bf16[128,256]{1,0:T(8,128)(2,1)S(1)}, bf16[128,256]{1,0:T(8,128)(2,1)S(1)}, u32[]{:S(2)}, u32[]{:S(2)}) collective-permute-start(bf16[128,256]{1,0:T(8,128)(2,1)S(1)} %bitcast.142), channel_id=1, source_target_pairs={{0,1},{1,0},{2,3},{3,2},{4,5},{5,4},{6,7},{7,6},{8,9},{9,8},{10,11... | collective-permute-start | bytes 196616 | tf_op jit(solution)/shard_map/ppermute | solution.py:34
  203.8 9.1 %collective-permute-start.2 = (bf16[128,256]{1,0:T(8,128)(2,1)S(1)}, bf16[128,256]{1,0:T(8,128)(2,1)S(1)}, u32[]{:S(2)}, u32[]{:S(2)}) collective-permute-start(bf16[128,256]{1,0:T(8,128)(2,1)S(1)} %bitcast.141), channel_id=1, source_target_pairs={{0,2},{1,3},{2,0},{3,1},{4,6},{5,7},{6,4},{7,5},{8,10},{9,11},{10,... | collective-permute-start | bytes 196616 | tf_op jit(solution)/shard_map/ppermute | solution.py:34
  205.5 7.9 %collective-permute-start.3 = (bf16[128,256]{1,0:T(8,128)(2,1)S(1)}, bf16[128,256]{1,0:T(8,128)(2,1)S(1)}, u32[]{:S(2)}, u32[]{:S(2)}) collective-permute-start(bf16[128,256]{1,0:T(8,128)(2,1)S(1)} %bitcast.140), channel_id=1, source_target_pairs={{0,3},{1,2},{2,1},{3,0},{4,7},{5,6},{6,5},{7,4},{8,11},{9,10},{10,... | collective-permute-start | bytes 196616 | tf_op jit(solution)/shard_map/ppermute | solution.py:34
  206.1 7.3 %collective-permute-start.4 = (bf16[128,256]{1,0:T(8,128)(2,1)S(1)}, bf16[128,256]{1,0:T(8,128)(2,1)S(1)}, u32[]{:S(2)}, u32[]{:S(2)}) collective-permute-start(bf16[128,256]{1,0:T(8,128)(2,1)S(1)} %bitcast.138), channel_id=1, source_target_pairs={{0,4},{1,5},{2,6},{3,7},{4,0},{5,1},{6,2},{7,3},{8,12},{9,13},{10,... | collective-permute-start | bytes 196616 | tf_op jit(solution)/shard_map/ppermute | solution.py:34
  209.5 5.9 %collective-permute-start.5 = (bf16[128,256]{1,0:T(8,128)(2,1)S(1)}, bf16[128,256]{1,0:T(8,128)(2,1)S(1)}, u32[]{:S(2)}, u32[]{:S(2)}) collective-permute-start(bf16[128,256]{1,0:T(8,128)(2,1)S(1)} %bitcast.137), channel_id=1, source_target_pairs={{0,5},{1,4},{2,7},{3,6},{4,1},{5,0},{6,3},{7,2},{8,13},{9,12},{10,... | collective-permute-start | bytes 196616 | tf_op jit(solution)/shard_map/ppermute | solution.py:34
  210.1 6.8 %collective-permute-start.6 = (bf16[128,256]{1,0:T(8,128)(2,1)S(1)}, bf16[128,256]{1,0:T(8,128)(2,1)S(1)}, u32[]{:S(2)}, u32[]{:S(2)}) collective-permute-start(bf16[128,256]{1,0:T(8,128)(2,1)S(1)} %bitcast.139), channel_id=1, source_target_pairs={{0,6},{1,7},{2,4},{3,5},{4,2},{5,3},{6,0},{7,1},{8,14},{9,15},{10,... | collective-permute-start | bytes 196616 | tf_op jit(solution)/shard_map/ppermute | solution.py:34
  213.0 5.3 %collective-permute-start.7 = (bf16[128,256]{1,0:T(8,128)(2,1)S(1)}, bf16[128,256]{1,0:T(8,128)(2,1)S(1)}, u32[]{:S(2)}, u32[]{:S(2)}) collective-permute-start(bf16[128,256]{1,0:T(8,128)(2,1)S(1)} %bitcast.136), channel_id=1, source_target_pairs={{0,7},{1,6},{2,5},{3,4},{4,3},{5,2},{6,1},{7,0},{8,15},{9,14},{10,... | collective-permute-start | bytes 196616 | tf_op jit(solution)/shard_map/ppermute | solution.py:34
  219.1 2.0 copy-start.18
  221.1 12.4 %copy-start.1 = (bf16[2048,512]{1,0:T(8,128)(2,1)S(1)}, bf16[2048,512]{1,0:T(8,128)(2,1)}, u32[]{:S(2)}) copy-start(bf16[2048,512]{1,0:T(8,128)(2,1)} %param.28) | copy-start | bytes 6291460
Sparse Core Ops, SparseCore 0:
  42.4 100.8 all-gather.2
  203.6 25.9 all-gather.4
